TPU v7x, 32 devices: a whole 2x2x4 slice. The times are simulated.
32 devices in a mesh: ep: 8 (over z, core), tp: 4 (over y, x).
Axes of the slice: x: 2, y: 2, z: 4, core: 2. Of those that a mesh axis runs over, the one named last changes fastest.
Arguments:
- resid: bfloat16 [32, 2048], P('ep', 'tp'), may hold values from -6 to 6
- cache_key: bfloat16 [32, 8, 224, 256], P(('ep', 'tp')), may hold values from -360 to 360
- cache_value: bfloat16 [32, 8, 224, 256], P(('ep', 'tp')), may hold values from -6 to 6
- lengths: int32 [32], P(('ep', 'tp')), may hold values from 28 to 224
- lambdas: float32 [8], replicated, may hold values from 0.3 to 0.8
- mix_gain: float32 [2048], replicated, may hold values from 0.1 to 1.9
- query_gain: float32 [128], replicated, may hold values from 0.1 to 1.9
- key_gain: float32 [128], replicated, may hold values from 0.1 to 1.9
- sub_gain: float32 [256], replicated, may hold values from 0.1 to 1.9
- ffn_gain: float32 [2048], replicated, may hold values from 0.1 to 1.9
- w_query: bfloat16 [2048, 2048], P(None, 'tp'), may hold values from -0.125 to 0.125
- w_key: bfloat16 [2048, 2048], P(None, 'tp'), may hold values from -0.125 to 0.125
- w_value: bfloat16 [2048, 2048], P(None, 'tp'), may hold values from -0.125 to 0.125
- w_out: bfloat16 [2048, 2048], P(None, 'tp'), may hold values from -0.125 to 0.125
- routes: int32 [32, 2], P('ep'), may hold values from 0 to 7, all different within a row; in each aligned block of 4 rows (0 to 3, 4 to 7, ...) at most 4 rows name the same one
- route_weights: float32 [32, 2], P('ep'), may hold values from 0.2 to 0.8
- w_gate: bfloat16 [8, 2048, 4096], P('ep', None, 'tp'), may hold values from -0.125 to 0.125
- w_up: bfloat16 [8, 2048, 4096], P('ep', None, 'tp'), may hold values from -0.125 to 0.125
- w_down: bfloat16 [8, 4096, 2048], P('ep', 'tp'), may hold values from -0.09375 to 0.09375
Outputs:
- result: bfloat16 [32, 2048], P('ep', 'tp')
- new_key: bfloat16 [32, 8, 256], P(('ep', 'tp'))
- new_value: bfloat16 [32, 8, 256], P(('ep', 'tp'))
Inputs may be any that keep to these rules, and one draw needn't show every extreme that they name: `routes`: within the 4 rows of one index of ep no expert is named more than 4 times, and in some of them one expert is named exactly 4 times; the two experts of a row differ. `lengths`: every sequence has at least two live positions.
All inputs are finite; a program needn't handle non-finite values.
Results may differ from a plain program's by a relative error of at most 0.0099.
Values may be sent and summed in bfloat16 or wider, within the bound.
A program may use at most 64 MiB of HBM per device.

v0:
```python
import math
import jax
import jax.numpy as jnp
from jax import lax
from jax.sharding import PartitionSpec as P

CAP = 4
epsilon = 1e-06
out_factor = 0.2 + 0.6 * math.exp(-0.3)
masked_score = -1e30


def scaled_rows(values, gain):
    wide = values.astype(jnp.float32)
    return wide * lax.rsqrt(jnp.mean(wide * wide, axis=-1, keepdims=True) + epsilon) * gain


def route_tables(routes, route_weights, experts, capacity):
    flat_routes = routes.reshape(-1)
    expert_hit = (flat_routes[:, None] == jnp.arange(experts, dtype=jnp.int32)[None, :]).astype(
        jnp.int32
    )
    before = jnp.cumsum(expert_hit, axis=0) - expert_hit
    slot_index = jnp.sum(before * expert_hit, axis=1)
    slot_hit = (slot_index[:, None] == jnp.arange(capacity, dtype=jnp.int32)[None, :]).astype(
        jnp.float32
    )
    pair_table = expert_hit.astype(jnp.float32)[:, :, None] * slot_hit[:, None, :]
    pair_table = pair_table.reshape(routes.shape[0], 2, experts, capacity)
    dispatch = jnp.sum(pair_table, axis=1)
    combine = jnp.sum(pair_table * route_weights[:, :, None, None], axis=1)
    return (dispatch, combine)


def attend(
    queries,
    key_rows,
    value_rows,
    past_keys,
    past_values,
    live_len,
    lambdas,
    query_gain,
    key_gain,
    sub_gain,
):
    seq_count, kv_heads, cache_len, key_width = past_keys.shape
    head_dim = key_width // 2
    head_count = lambdas.shape[0]
    group_size = head_count // kv_heads
    value_dim = past_values.shape[-1]
    score_scale = head_dim ** (-0.5)
    q_unit = scaled_rows(
        queries.reshape(seq_count, kv_heads, group_size, 2, head_dim), query_gain
    ).astype(jnp.bfloat16)
    new_key = scaled_rows(key_rows.reshape(seq_count, kv_heads, 2, head_dim), key_gain).astype(
        jnp.bfloat16
    )
    new_value = value_rows.reshape(seq_count, kv_heads, value_dim)
    past_split = past_keys.reshape(seq_count, kv_heads, cache_len, 2, head_dim)
    scores = (
        jnp.einsum("sjgmd,sjlmd->sjgml", q_unit, past_split, preferred_element_type=jnp.float32)
        * score_scale
    )
    own_score = (
        jnp.einsum("sjgmd,sjmd->sjgm", q_unit, new_key, preferred_element_type=jnp.float32)
        * score_scale
    )
    live_mask = jnp.arange(cache_len, dtype=jnp.int32)[None, :] < live_len[:, None]
    scores = jnp.where(live_mask[:, None, None, None, :], scores, masked_score)
    peak = jnp.maximum(jnp.max(scores, axis=-1), own_score)
    past_weight = jnp.exp(scores - peak[..., None])
    own_weight = jnp.exp(own_score - peak)
    totals = jnp.sum(past_weight, axis=-1) + own_weight
    past_prob = past_weight / totals[..., None]
    own_prob = own_weight / totals
    mix_lambda = lambdas.reshape(1, kv_heads, group_size, 1)
    past_mix = (past_prob[..., 0, :] - mix_lambda * past_prob[..., 1, :]).astype(jnp.bfloat16)
    own_mix = (own_prob[..., 0] - mix_lambda[..., 0] * own_prob[..., 1]).astype(jnp.bfloat16)
    head_out = jnp.einsum(
        "sjgl,sjlv->sjgv", past_mix, past_values, preferred_element_type=jnp.float32
    )
    head_out = (
        head_out
        + own_mix.astype(jnp.float32)[..., None] * new_value.astype(jnp.float32)[:, :, None, :]
    )
    mixed = (
        (scaled_rows(head_out, sub_gain) * out_factor)
        .astype(jnp.bfloat16)
        .reshape(seq_count, head_count * value_dim)
    )
    return (mixed, new_key.reshape(seq_count, kv_heads, key_width), new_value)


def local(
    resid,
    cache_key,
    cache_value,
    lengths,
    lambdas,
    mix_gain,
    query_gain,
    key_gain,
    sub_gain,
    ffn_gain,
    w_query,
    w_key,
    w_value,
    w_out,
    routes,
    route_weights,
    w_gate,
    w_up,
    w_down,
):
    gathered = lax.all_gather(resid, "tp", axis=1, tiled=True)
    normed = scaled_rows(gathered, mix_gain).astype(jnp.bfloat16)
    query_part = jnp.dot(normed, w_query, preferred_element_type=jnp.float32).astype(jnp.bfloat16)
    key_part = jnp.dot(normed, w_key, preferred_element_type=jnp.float32).astype(jnp.bfloat16)
    value_part = jnp.dot(normed, w_value, preferred_element_type=jnp.float32).astype(jnp.bfloat16)
    queries, key_rows, value_rows = (
        lax.all_to_all(query_part, "tp", split_axis=0, concat_axis=1, tiled=True),
        lax.all_to_all(key_part, "tp", split_axis=0, concat_axis=1, tiled=True),
        lax.all_to_all(value_part, "tp", split_axis=0, concat_axis=1, tiled=True),
    )
    mixed, new_key, new_value = attend(
        queries,
        key_rows,
        value_rows,
        cache_key,
        cache_value,
        lengths,
        lambdas,
        query_gain,
        key_gain,
        sub_gain,
    )
    attn_proj = jnp.dot(
        lax.all_gather(mixed, "tp", axis=0, tiled=True), w_out, preferred_element_type=jnp.float32
    )
    updated = (resid.astype(jnp.float32) + attn_proj).astype(jnp.bfloat16)
    updated_rows = lax.all_gather(updated, "tp", axis=1, tiled=True)
    hidden = scaled_rows(updated_rows, ffn_gain).astype(jnp.bfloat16)
    experts = w_gate.shape[0] * lax.axis_size("ep")
    dispatch, combine = route_tables(routes, route_weights, experts, CAP)
    send = jnp.einsum(
        "gec,gd->ecd", dispatch.astype(jnp.bfloat16), hidden, preferred_element_type=jnp.float32
    ).astype(jnp.bfloat16)
    slots = lax.all_to_all(send, "ep", split_axis=0, concat_axis=0, tiled=True)
    flat_rows = slots.reshape(-1, slots.shape[-1])
    gate_out = jnp.dot(flat_rows, w_gate[0], preferred_element_type=jnp.float32)
    up_out = jnp.dot(flat_rows, w_up[0], preferred_element_type=jnp.float32)
    act = (jax.nn.silu(gate_out) * up_out).astype(jnp.bfloat16)
    down_out = jnp.dot(act, w_down[0], preferred_element_type=jnp.float32)
    partial_value = down_out.reshape(slots.shape[0], slots.shape[1], down_out.shape[-1])
    flat_combine = combine.reshape(combine.shape[0], -1)
    summed = lax.psum_scatter(
        partial_value.astype(jnp.bfloat16), "tp", scatter_dimension=2, tiled=True
    ).astype(jnp.float32)
    returned = lax.all_to_all(
        summed.astype(jnp.bfloat16), "ep", split_axis=0, concat_axis=0, tiled=True
    ).astype(summed.dtype)
    expert_mix = jnp.dot(
        flat_combine,
        returned.reshape(-1, returned.shape[-1]),
        precision=lax.Precision.HIGHEST,
        preferred_element_type=jnp.float32,
    )
    result = (updated.astype(jnp.float32) + expert_mix).astype(jnp.bfloat16)
    return (result, new_key, new_value)


def solution(mesh):
    in_specs = (
        P("ep", "tp"),
        P(("ep", "tp"), None, None, None),
        P(("ep", "tp"), None, None, None),
        P(("ep", "tp")),
        P(),
        P(),
        P(),
        P(),
        P(),
        P(),
        P(None, "tp"),
        P(None, "tp"),
        P(None, "tp"),
        P(None, "tp"),
        P("ep", None),
        P("ep", None),
        P("ep", None, "tp"),
        P("ep", None, "tp"),
        P("ep", "tp", None),
    )
    out_specs = (P("ep", "tp"), P(("ep", "tp"), None, None), P(("ep", "tp"), None, None))
    return jax.shard_map(local, mesh=mesh, in_specs=in_specs, out_specs=out_specs, check_vma=False)
```

profile of v0, /device:TPU:0, one launch (start us, length us, event | category | flops | bytes accessed | tf_op | source)
XLA Modules:
  0.0 129.9 jit_solution(2296652605895860037)
XLA Ops:
  7.2 0.0 copy-start
  7.2 0.0 copy-start.3
  7.2 9.9 %all_gather.9 = bf16[4,2048]{1,0:T(4,128)(2,1)S(1)} all-gather(bf16[4,512]{1,0:T(4,128)(2,1)} %param.19), channel_id=1, replica_groups=mesh['ep'=8,'tp'=4] {'tp'}, dimensions={1}, use_global_device_ids=true | all-gather | bytes 20480 | tf_op jit(solution)/shard_map/all_gather | solution.py:116
  17.1 0.1 fusion.26
  17.3 1.1 fusion.18
  18.4 0.5 broadcast.214
  18.9 0.7 reduce.19
  19.6 0.6 reshape.382
  20.2 3.2 %all-to-all-start = ((bf16[4,2,256]{2,1,0:T(2,128)(2,1)}), bf16[4,2,256]{2,1,0:T(2,128)(2,1)S(1)}, u32[]{:S(2)}, u32[]{:S(2)}) async-start(bf16[4,2,256]{2,1,0:T(2,128)(2,1)} %reshape.382), calls=%async_computation | async-start | bytes 8192 | tf_op jit(solution)/shard_map/all_to_all | solution.py:122
  23.4 0.1 copy.64
  23.5 0.1 eq.47
  23.6 0.1 fusion.48
  23.7 2.1 %fusion.19 = bf16[4,1,512]{2,0,1:T(4,128)(2,1)S(1)} fusion(bf16[2048,512]{1,0:T(8,128)(2,1)} %param.30, bf16[4,2048]{1,0:T(4,128)(2,1)S(1)} %all_gather.9, f32[2048]{0:T(1024)S(1)} %copy-done.3, f32[4]{0:T(128)S(1)} %add_rsqrt_fusion.4), kind=kOutput, calls=%fused_computation.19 | convolution fusion | flops 8423424 | bytes 2125840 | tf_op jit(solution)/shard_map/dot_general | solution.py:119
  26.5 0.0 copy-start.10
  26.5 0.4 fusion.20
  27.0 0.1 fusion.51
  27.1 0.2 select_reduce_fusion
  27.2 0.1 eq.51
  27.3 0.1 compare_convert_fusion
  27.4 0.1 copy.66
  27.5 0.1 multiply_reduce_fusion
  27.6 0.7 reduce.18
  28.3 0.6 reshape.384
  28.9 2.2 %reshape.356 = bf16[8,224,2,128]{3,2,1,0:T(2,128)(2,1)S(1)} reshape(bf16[1,8,224,256]{3,2,1,0:T(8,128)(2,1)} %param.20) | data formatting | bytes 1835008 | tf_op jit(solution)/shard_map/reshape.7
  31.1 0.7 reduce.17
  31.7 0.6 reshape.380
  32.3 4.2 %all-to-all-start.1 = ((bf16[4,2,256]{2,1,0:T(2,128)(2,1)}), bf16[4,2,256]{2,1,0:T(2,128)(2,1)S(1)}, u32[]{:S(2)}, u32[]{:S(2)}) async-start(bf16[4,2,256]{2,1,0:T(2,128)(2,1)} %reshape.384), calls=%async_computation.1 | async-start | bytes 8192 | tf_op jit(solution)/shard_map/all_to_all | solution.py:123
  36.5 4.6 %all-to-all-done.1 = bf16[4,2,256]{2,1,0:T(2,128)(2,1)S(1)} async-done(((bf16[4,2,256]{2,1,0:T(2,128)(2,1)}), bf16[4,2,256]{2,1,0:T(2,128)(2,1)S(1)}, u32[]{:S(2)}, u32[]{:S(2)}) %all-to-all-start.1) | async-done | bytes 4128 | tf_op jit(solution)/shard_map/all_to_all | solution.py:123
  41.2 3.2 %all-to-all-start.2 = ((bf16[4,2,256]{2,1,0:T(2,128)(2,1)}), bf16[4,2,256]{2,1,0:T(2,128)(2,1)S(1)}, u32[]{:S(2)}, u32[]{:S(2)}) async-start(bf16[4,2,256]{2,1,0:T(2,128)(2,1)} %reshape.380), calls=%async_computation.2 | async-start | bytes 8192 | tf_op jit(solution)/shard_map/all_to_all | solution.py:124
  44.4 0.0 reduce-scatter.2.cloned.1.call-start
  44.6 0.1 reduce_sum.83
  44.6 0.1 reduce_sum.82
  44.8 0.2 fusion.45
  44.9 0.1 copy.79
  45.0 0.6 fusion.23
  45.6 0.1 fusion.41
  45.7 0.2 fusion.40
  45.9 0.1 divide_bitcast_fusion
  46.0 0.1 fusion.49
  46.1 3.0 %all-to-all-done.2 = bf16[4,2,256]{2,1,0:T(2,128)(2,1)S(1)} async-done(((bf16[4,2,256]{2,1,0:T(2,128)(2,1)}), bf16[4,2,256]{2,1,0:T(2,128)(2,1)S(1)}, u32[]{:S(2)}, u32[]{:S(2)}) %all-to-all-start.2) | async-done | bytes 4128 | tf_op jit(solution)/shard_map/all_to_all | solution.py:124
  49.1 1.4 %fusion.21 = f32[8,1,256]{2,1,0:T(1,128)S(1)} fusion(bf16[1,8,224,256]{3,2,1,0:T(8,128)(2,1)} %param.21, bf16[8,224,1]{1,0,2:T(8,128)(2,1)S(1)} %fusion.49), kind=kOutput, calls=%fused_computation.21 | convolution fusion | flops 917504 | bytes 929280 | tf_op jit(solution)/shard_map/sjgl,sjlv->sjgv/dot_general | solution.py:80
  50.5 0.2 multiply_reduce_fusion.1
  50.8 0.1 multiply_convert_fusion.1
  50.8 7.2 %all-gather = bf16[4,1,2048]{2,1,0:T(2,128)(2,1)S(1)} all-gather(bf16[1,1,2048]{2,1,0:T(2,128)(2,1)S(1)} %reshape.365), channel_id=1, replica_groups=mesh['ep'=8,'tp'=4] {'tp'}, dimensions={0}, use_global_device_ids=true | all-gather | bytes 20480 | tf_op jit(solution)/shard_map/all_gather | solution.py:139
  58.1 2.0 %fusion.15 = bf16[4,512]{1,0:T(4,128)(2,1)S(1)} fusion(bf16[2048,512]{1,0:T(8,128)(2,1)} %param.32, bf16[4,1,2048]{2,1,0:T(2,128)(2,1)S(1)} %all-gather, bf16[4,512]{1,0:T(4,128)(2,1)S(1)} %copy-done.4), kind=kOutput, calls=%fused_computation.12 | convolution fusion | flops 8394752 | bytes 2121728 | tf_op jit(solution)/shard_map/dot_general | solution.py:138
  60.1 8.1 %all_gather.11 = bf16[4,2048]{1,0:T(4,128)(2,1)S(1)} all-gather(bf16[4,512]{1,0:T(4,128)(2,1)S(1)} %fusion.15), channel_id=1, replica_groups=mesh['ep'=8,'tp'=4] {'tp'}, dimensions={1}, use_global_device_ids=true | all-gather | bytes 20480 | tf_op jit(solution)/shard_map/all_gather | solution.py:142
  68.2 0.1 fusion.29
  68.3 0.2 convolution_convert_fusion
  68.6 0.1 copy.68
  68.7 11.4 %all_to_all.49 = bf16[8,4,2048]{2,1,0:T(4,128)(2,1)S(1)} all-to-all(bf16[8,4,2048]{2,1,0:T(4,128)(2,1)S(1)} %copy.68), channel_id=1, replica_groups=mesh['ep'=8,'tp'=4] {'ep'}, dimensions={0} | all-to-all | bytes 262144 | tf_op jit(solution)/shard_map/all_to_all | solution.py:149
  80.2 3.2 %fusion.4 = f32[32,1024]{1,0:T(8,128)S(1)} fusion(bf16[32,2048]{1,0:T(8,128)(2,1)S(1)} %reshape.359, bf16[1,2048,1024]{2,1,0:T(8,128)(2,1)} %param.35), kind=kOutput, calls=%fused_computation.4 | convolution fusion | flops 134217728 | bytes 4456448 | tf_op jit(solution)/shard_map/dot_general | solution.py:151
  83.3 0.3 copy-done.1
  83.6 0.8 fusion.12
  84.5 3.6 %fusion.6 = bf16[8,4,2048]{2,0,1:T(8,128)(2,1)} fusion(bf16[1,1024,2048]{2,1,0:T(8,128)(2,1)} %param.37, bf16[8,4,1024]{2,1,0:T(4,128)(2,1)S(1)} %dot_general.48), kind=kOutput, calls=%fused_computation.6 | convolution fusion | flops 134283264 | bytes 4390912 | tf_op jit(solution)/shard_map/dot_general | solution.py:154
  88.1 0.0 reduce-scatter.2.cloned.1.call-update
  88.1 0.1 copy.82
  88.2 0.1 mul.249
  88.3 22.2 %reduce-scatter.2.cloned.1.call-done = bf16[8,4,512]{2,0,1:T(8,128)(2,1)} async-done(((bf16[8,4,2048]{2,0,1:T(8,128)(2,1)}), bf16[8,4,512]{2,0,1:T(8,128)(2,1)}) %reduce-scatter.2.cloned.1.call-update) | async-done | bytes 32784 | tf_op jit(solution)/shard_map/reduce_scatter | solution.py:157
  110.5 1.4 %copy.70 = bf16[8,4,512]{2,1,0:T(4,128)(2,1)} copy(bf16[8,4,512]{2,0,1:T(8,128)(2,1)} %reduce-scatter.2.cloned.1.call-done) | data formatting | bytes 65536 | tf_op jit(solution)/shard_map/reduce_scatter | solution.py:157
  111.9 4.6 %all-to-all-start.4 = ((bf16[8,4,512]{2,1,0:T(4,128)(2,1)}), bf16[8,4,512]{2,1,0:T(4,128)(2,1)S(1)}, u32[]{:S(2)}, u32[]{:S(2)}) async-start(bf16[8,4,512]{2,1,0:T(4,128)(2,1)} %copy.70), calls=%async_computation.5 | async-start | bytes 65536 | tf_op jit(solution)/shard_map/all_to_all | solution.py:160
  116.5 0.6 multiply_convert_fusion
  117.1 0.6 reshape.360
  117.7 4.5 %all-to-all-done.4 = bf16[8,4,512]{2,1,0:T(4,128)(2,1)S(1)} async-done(((bf16[8,4,512]{2,1,0:T(4,128)(2,1)}), bf16[8,4,512]{2,1,0:T(4,128)(2,1)S(1)}, u32[]{:S(2)}, u32[]{:S(2)}) %all-to-all-start.4) | async-done | bytes 32800 | tf_op jit(solution)/shard_map/all_to_all | solution.py:160
  122.2 0.8 fusion.17
  (46 shorter events, 0.4 us)
Async XLA Ops:
  7.2 10.1 %copy-start = (bf16[2048,512]{1,0:T(8,128)(2,1)S(1)}, bf16[2048,512]{1,0:T(8,128)(2,1)}, u32[]{:S(2)}) copy-start(bf16[2048,512]{1,0:T(8,128)(2,1)} %param.29) | copy-start | bytes 6291460
  7.2 16.5 %copy-start.3 = (f32[2048]{0:T(1024)S(1)}, f32[2048]{0:T(1024)}, u32[]{:S(2)}) copy-start(f32[2048]{0:T(1024)} %param.24) | copy-start | bytes 24580
  7.2 16.2 %copy-start.7 = (s32[4,2]{0,1:T(2,128)S(1)}, s32[4,2]{0,1:T(2,128)}, u32[]{:S(2)}) copy-start(s32[4,2]{0,1:T(2,128)} %param.33) | copy-start | bytes 100
  20.2 12.2 %all-to-all-start = ((bf16[4,2,256]{2,1,0:T(2,128)(2,1)}), bf16[4,2,256]{2,1,0:T(2,128)(2,1)S(1)}, u32[]{:S(2)}, u32[]{:S(2)}) async-start(bf16[4,2,256]{2,1,0:T(2,128)(2,1)} %reshape.382), calls=%async_computation | async-start | bytes 8192 | tf_op jit(solution)/shard_map/all_to_all | solution.py:122
  23.6 2.9 %copy-start.2 = (bf16[2048,512]{1,0:T(8,128)(2,1)S(1)}, bf16[2048,512]{1,0:T(8,128)(2,1)}, u32[]{:S(2)}) copy-start(bf16[2048,512]{1,0:T(8,128)(2,1)} %param.31) | copy-start | bytes 6291460
  23.7 3.7 %copy-start.8 = (f32[4,2]{0,1:T(2,128)S(1)}, f32[4,2]{0,1:T(2,128)}, u32[]{:S(2)}) copy-start(f32[4,2]{0,1:T(2,128)} %param.34) | copy-start | bytes 100
  26.5 18.2 %copy-start.10 = (f32[128]{0:T(128)S(1)}, f32[128]{0:T(128)}, u32[]{:S(2)}) copy-start(f32[128]{0:T(128)} %param.25) | copy-start | bytes 1540
  26.5 18.2 %copy-start.11 = (f32[128]{0:T(128)S(1)}, f32[128]{0:T(128)}, u32[]{:S(2)}) copy-start(f32[128]{0:T(128)} %param.26) | copy-start | bytes 1540
  27.0 19.0 %copy-start.6 = (f32[8]{0:T(128)S(1)}, f32[8]{0:T(128)}, u32[]{:S(2)}) copy-start(f32[8]{0:T(128)} %param.23) | copy-start | bytes 100
  27.0 23.8 %copy-start.9 = (f32[256]{0:T(256)S(1)}, f32[256]{0:T(256)}, u32[]{:S(2)}) copy-start(f32[256]{0:T(256)} %param.27) | copy-start | bytes 3076
  28.9 29.2 %copy-start.4 = (bf16[4,512]{1,0:T(4,128)(2,1)S(1)}, bf16[4,512]{1,0:T(4,128)(2,1)}, u32[]{:S(2)}) copy-start(bf16[4,512]{1,0:T(4,128)(2,1)} %param.19) | copy-start | bytes 12292
  32.3 8.8 %all-to-all-start.1 = ((bf16[4,2,256]{2,1,0:T(2,128)(2,1)}), bf16[4,2,256]{2,1,0:T(2,128)(2,1)S(1)}, u32[]{:S(2)}, u32[]{:S(2)}) async-start(bf16[4,2,256]{2,1,0:T(2,128)(2,1)} %reshape.384), calls=%async_computation.1 | async-start | bytes 8192 | tf_op jit(solution)/shard_map/all_to_all | solution.py:123
  41.2 7.9 %all-to-all-start.2 = ((bf16[4,2,256]{2,1,0:T(2,128)(2,1)}), bf16[4,2,256]{2,1,0:T(2,128)(2,1)S(1)}, u32[]{:S(2)}, u32[]{:S(2)}) async-start(bf16[4,2,256]{2,1,0:T(2,128)(2,1)} %reshape.380), calls=%async_computation.2 | async-start | bytes 8192 | tf_op jit(solution)/shard_map/all_to_all | solution.py:124
  44.4 66.1 %reduce-scatter.2.cloned.1.call-start = ((), (), s32[]{:S(2)}) async-start(), calls=%async_computation.6 | async-start | bytes 163840 | tf_op jit(solution)/shard_map/reduce_scatter | solution.py:157
  45.0 23.3 %copy-start.5 = (f32[2048]{0:T(1024)S(1)}, f32[2048]{0:T(1024)}, u32[]{:S(2)}) copy-start(f32[2048]{0:T(1024)} %param.28) | copy-start | bytes 24580
  80.2 3.5 %copy-start.1 = (bf16[1,2048,1024]{2,1,0:T(8,128)(2,1)S(1)}, bf16[1,2048,1024]{2,1,0:T(8,128)(2,1)}, u32[]{:S(2)}) copy-start(bf16[1,2048,1024]{2,1,0:T(8,128)(2,1)} %param.36) | copy-start | bytes 12582916
  111.9 10.3 %all-to-all-start.4 = ((bf16[8,4,512]{2,1,0:T(4,128)(2,1)}), bf16[8,4,512]{2,1,0:T(4,128)(2,1)S(1)}, u32[]{:S(2)}, u32[]{:S(2)}) async-start(bf16[8,4,512]{2,1,0:T(4,128)(2,1)} %copy.70), calls=%async_computation.5 | async-start | bytes 65536 | tf_op jit(solution)/shard_map/all_to_all | solution.py:160
Sparse Core Ops, SparseCore 0:
  88.2 22.2 reduce-scatter.1
where the time goes:
time: 131 us; the launch traced here: 130 us
  blocking collectives  36.7 us (28%)
  waiting for transfers between devices  34.4 us (26%)
  matrix products  16.3 us (12%)
  starting transfers between devices  15.3 us (12%)
  between operations  15 us (11%)
  local copies, waits for them, and re-layouts  7.69 us (6%)
  other arithmetic  4.59 us (4%)
    reduce_scatter x1, waiting for transfers between devices, local(): lax.psum_scatter(partial_value.astype(jnp.bfloat16), 'tp', scatter_dimens...  22.2 us
    all_to_all x1, blocking collectives, local(): slots = lax.all_to_all(send, 'ep', split_axis=0, concat_axis=0, tiled=True)  11.4 us
    all_gather x1, blocking collectives, local(): gathered = lax.all_gather(resid, 'tp', axis=1, tiled=True)  9.93 us
    all_gather x1, blocking collectives, local(): updated_rows = lax.all_gather(updated, 'tp', axis=1, tiled=True)  8.12 us
    all_gather x1, blocking collectives, local(): lax.all_gather(mixed, 'tp', axis=0, tiled=True)  7.25 us
    all_to_all x1, waiting for transfers between devices, local(): lax.all_to_all(key_part, 'tp', split_axis=0, concat_axis=1, tiled=True)  4.63 us
    all_to_all x1, starting transfers between devices, local(): lax.all_to_all(summed.astype(jnp.bfloat16), 'ep', split_axis=0, concat_ax...  4.6 us
    all_to_all x1, waiting for transfers between devices, local(): lax.all_to_all(summed.astype(jnp.bfloat16), 'ep', split_axis=0, concat_ax...  4.51 us
  transfers between devices with their start and end apart: 5, of which 4 were waited for; matrix products, arithmetic and copies ran while one was open for 9% of the time, Pallas kernels for 0%

commit v1 on v0

--- a/solution.py
+++ b/solution.py
@@ -113,7 +113,11 @@
     w_up,
     w_down,
 ):
-    gathered = lax.all_gather(resid, "tp", axis=1, tiled=True)
+
+    def name_spots_on(row_data, dim_no):
+        return jnp.concatenate(lax.all_gather(row_data, "tp"), dim_no)
+
+    gathered = name_spots_on(resid, 1)
     normed = scaled_rows(gathered, mix_gain).astype(jnp.bfloat16)
     query_part = jnp.dot(normed, w_query, preferred_element_type=jnp.float32).astype(jnp.bfloat16)
     key_part = jnp.dot(normed, w_key, preferred_element_type=jnp.float32).astype(jnp.bfloat16)

time: 131 us -> 131 us (level)
    all_to_all x1, waiting for transfers between devices: 4.63 us -> 0.01 us  [local(): lax.all_to_all(key_part, 'tp', split_axis=0, concat_axis=1, tiled=True)]
    all_to_all x1, waiting for transfers between devices: 0.01 us -> 4.61 us  [local(): lax.all_to_all(query_part, 'tp', split_axis=0, concat_axis=1, tiled=True)]
    dot_general x1, matrix products: 2.14 us -> 0.37 us  [local(): jnp.dot(normed, w_key, preferred_element_type=jnp.float32)]
  transfers between devices with their start and end apart: 5 -> 5, of which waited for: 4 -> 4; matrix products, arithmetic and copies ran while one was open for 9% -> 8% of each run, Pallas kernels for 0% -> 0%
where the time goes in v1:
time: 131 us; the launch traced here: 130 us
  blocking collectives  36.7 us (28%)
  waiting for transfers between devices  34.4 us (26%)
  matrix products  15.4 us (12%)
  starting transfers between devices  15.3 us (12%)
  between operations  15 us (11%)
  local copies, waits for them, and re-layouts  7.69 us (6%)
  other arithmetic  5.37 us (4%)
    reduce_scatter x1, waiting for transfers between devices, local(): lax.psum_scatter(partial_value.astype(jnp.bfloat16), 'tp', scatter_dimens...  22.2 us
    all_to_all x1, blocking collectives, local(): slots = lax.all_to_all(send, 'ep', split_axis=0, concat_axis=0, tiled=True)  11.4 us
    all_gather x1, blocking collectives, name_spots_on(): return jnp.concatenate(lax.all_gather(row_data, 'tp'), dim_no)  9.93 us
    all_gather x1, blocking collectives, local(): updated_rows = lax.all_gather(updated, 'tp', axis=1, tiled=True)  8.12 us
    all_gather x1, blocking collectives, local(): lax.all_gather(mixed, 'tp', axis=0, tiled=True)  7.25 us
    all_to_all x1, waiting for transfers between devices, local(): lax.all_to_all(query_part, 'tp', split_axis=0, concat_axis=1, tiled=True)  4.61 us
    all_to_all x1, starting transfers between devices, local(): lax.all_to_all(summed.astype(jnp.bfloat16), 'ep', split_axis=0, concat_ax...  4.6 us
    all_to_all x1, waiting for transfers between devices, local(): lax.all_to_all(summed.astype(jnp.bfloat16), 'ep', split_axis=0, concat_ax...  4.51 us
  transfers between devices with their start and end apart: 5, of which 4 were waited for; matrix products, arithmetic and copies ran while one was open for 8% of the time, Pallas kernels for 0%

profile of v1, /device:TPU:0, one launch (start us, length us, event | category | flops | bytes accessed | tf_op | source)
XLA Modules:
  0.0 129.9 jit_solution(7970023615273310814)
XLA Ops:
  7.2 0.0 copy-start
  7.2 9.9 %all-gather.1 = bf16[4,4,512]{2,1,0:T(4,128)(2,1)S(1)} all-gather(bf16[1,4,512]{2,1,0:T(4,128)(2,1)} %bitcast.117), channel_id=2, replica_groups=mesh['ep'=8,'tp'=4] {'tp'}, dimensions={0}, use_global_device_ids=true | all-gather | bytes 20480 | tf_op jit(solution)/shard_map/all_gather | solution.py:118
  17.1 0.1 multiply_reduce_fusion
  17.3 0.8 multiply_convert_fusion
  18.1 0.4 fusion.19
  18.4 0.5 broadcast.214
  19.0 0.7 reduce.20
  19.6 0.6 reshape.396
  20.2 3.2 %all-to-all-start.1 = ((bf16[4,2,256]{2,1,0:T(2,128)(2,1)}), bf16[4,2,256]{2,1,0:T(2,128)(2,1)S(1)}, u32[]{:S(2)}, u32[]{:S(2)}) async-start(bf16[4,2,256]{2,1,0:T(2,128)(2,1)} %reshape.396), calls=%async_computation.1 | async-start | bytes 8192 | tf_op jit(solution)/shard_map/all_to_all | solution.py:127
  23.5 0.1 copy.64
  23.6 0.1 eq.47
  23.7 0.1 fusion.45
  23.7 2.1 %fusion.18 = bf16[4,1,512]{2,0,1:T(4,128)(2,1)S(1)} fusion(bf16[4,2048]{1,0:T(4,128)(2,1)S(1)} %multiply_convert_fusion, bf16[2048,512]{1,0:T(8,128)(2,1)} %param.29), kind=kOutput, calls=%fused_computation.18 | convolution fusion | flops 8390656 | bytes 2117632 | tf_op jit(solution)/shard_map/dot_general | solution.py:122
  26.5 0.0 copy-start.9
  26.5 0.4 fusion.20
  26.9 0.1 fusion.48
  27.0 0.2 select_reduce_fusion
  27.2 0.1 eq.51
  27.3 0.1 compare_convert_fusion
  27.4 0.1 copy.66
  27.5 0.1 multiply_reduce_fusion.1
  27.6 0.7 reduce.21
  28.3 0.6 reshape.394
  28.9 2.2 %reshape.360 = bf16[8,224,2,128]{3,2,1,0:T(2,128)(2,1)S(1)} reshape(bf16[1,8,224,256]{3,2,1,0:T(8,128)(2,1)} %param.20) | data formatting | bytes 1835008 | tf_op jit(solution)/shard_map/reshape.7
  31.0 0.7 reduce.19
  31.7 0.6 reshape.392
  32.3 4.2 %all-to-all-start = ((bf16[4,2,256]{2,1,0:T(2,128)(2,1)}), bf16[4,2,256]{2,1,0:T(2,128)(2,1)S(1)}, u32[]{:S(2)}, u32[]{:S(2)}) async-start(bf16[4,2,256]{2,1,0:T(2,128)(2,1)} %reshape.394), calls=%async_computation | async-start | bytes 8192 | tf_op jit(solution)/shard_map/all_to_all | solution.py:126
  36.5 4.6 %all-to-all-done = bf16[4,2,256]{2,1,0:T(2,128)(2,1)S(1)} async-done(((bf16[4,2,256]{2,1,0:T(2,128)(2,1)}), bf16[4,2,256]{2,1,0:T(2,128)(2,1)S(1)}, u32[]{:S(2)}, u32[]{:S(2)}) %all-to-all-start) | async-done | bytes 4128 | tf_op jit(solution)/shard_map/all_to_all | solution.py:126
  41.1 3.2 %all-to-all-start.2 = ((bf16[4,2,256]{2,1,0:T(2,128)(2,1)}), bf16[4,2,256]{2,1,0:T(2,128)(2,1)S(1)}, u32[]{:S(2)}, u32[]{:S(2)}) async-start(bf16[4,2,256]{2,1,0:T(2,128)(2,1)} %reshape.392), calls=%async_computation.2 | async-start | bytes 8192 | tf_op jit(solution)/shard_map/all_to_all | solution.py:128
  44.4 0.0 reduce-scatter.2.cloned.1.call-start
  44.5 0.1 reduce_sum.83
  44.6 0.1 reduce_sum.82
  44.7 0.2 fusion.42
  44.9 0.1 copy.79
  45.0 0.6 fusion.23
  45.5 0.1 fusion.38
  45.6 0.2 fusion.37
  45.8 0.1 divide_bitcast_fusion
  45.9 0.1 fusion.46
  46.0 3.0 %all-to-all-done.2 = bf16[4,2,256]{2,1,0:T(2,128)(2,1)S(1)} async-done(((bf16[4,2,256]{2,1,0:T(2,128)(2,1)}), bf16[4,2,256]{2,1,0:T(2,128)(2,1)S(1)}, u32[]{:S(2)}, u32[]{:S(2)}) %all-to-all-start.2) | async-done | bytes 4128 | tf_op jit(solution)/shard_map/all_to_all | solution.py:128
  49.1 1.4 %fusion.21 = f32[8,1,256]{2,1,0:T(1,128)S(1)} fusion(bf16[1,8,224,256]{3,2,1,0:T(8,128)(2,1)} %param.21, bf16[8,224,1]{1,0,2:T(8,128)(2,1)S(1)} %fusion.46), kind=kOutput, calls=%fused_computation.21 | convolution fusion | flops 917504 | bytes 929280 | tf_op jit(solution)/shard_map/sjgl,sjlv->sjgv/dot_general | solution.py:80
  50.5 0.2 multiply_reduce_fusion.2
  50.7 0.1 multiply_convert_fusion.2
  50.8 7.2 %all-gather.2 = bf16[4,1,2048]{2,1,0:T(2,128)(2,1)S(1)} all-gather(bf16[1,1,2048]{2,1,0:T(2,128)(2,1)S(1)} %reshape.375), channel_id=1, replica_groups=mesh['ep'=8,'tp'=4] {'tp'}, dimensions={0}, use_global_device_ids=true | all-gather | bytes 20480 | tf_op jit(solution)/shard_map/all_gather | solution.py:143
  58.1 2.0 %fusion.15 = bf16[4,512]{1,0:T(4,128)(2,1)S(1)} fusion(bf16[2048,512]{1,0:T(8,128)(2,1)} %param.32, bf16[4,1,2048]{2,1,0:T(2,128)(2,1)S(1)} %all-gather.2, bf16[4,512]{1,0:T(4,128)(2,1)S(1)} %copy-done.3), kind=kOutput, calls=%fused_computation.12 | convolution fusion | flops 8394752 | bytes 2121728 | tf_op jit(solution)/shard_map/dot_general | solution.py:142
  60.0 8.1 %all_gather.15 = bf16[4,2048]{1,0:T(4,128)(2,1)S(1)} all-gather(bf16[4,512]{1,0:T(4,128)(2,1)S(1)} %fusion.15), channel_id=1, replica_groups=mesh['ep'=8,'tp'=4] {'tp'}, dimensions={1}, use_global_device_ids=true | all-gather | bytes 20480 | tf_op jit(solution)/shard_map/all_gather | solution.py:146
  68.2 0.1 fusion.26
  68.3 0.2 convolution_convert_fusion
  68.5 0.1 copy.68
  68.7 11.4 %all_to_all.49 = bf16[8,4,2048]{2,1,0:T(4,128)(2,1)S(1)} all-to-all(bf16[8,4,2048]{2,1,0:T(4,128)(2,1)S(1)} %copy.68), channel_id=1, replica_groups=mesh['ep'=8,'tp'=4] {'ep'}, dimensions={0} | all-to-all | bytes 262144 | tf_op jit(solution)/shard_map/all_to_all | solution.py:153
  80.1 3.2 %fusion.4 = f32[32,1024]{1,0:T(8,128)S(1)} fusion(bf16[32,2048]{1,0:T(8,128)(2,1)S(1)} %reshape.363, bf16[1,2048,1024]{2,1,0:T(8,128)(2,1)} %param.35), kind=kOutput, calls=%fused_computation.4 | convolution fusion | flops 134217728 | bytes 4456448 | tf_op jit(solution)/shard_map/dot_general | solution.py:155
  83.3 0.3 copy-done.1
  83.6 0.8 fusion.12
  84.4 3.6 %fusion.6 = bf16[8,4,2048]{2,0,1:T(8,128)(2,1)} fusion(bf16[1,1024,2048]{2,1,0:T(8,128)(2,1)} %param.37, bf16[8,4,1024]{2,1,0:T(4,128)(2,1)S(1)} %dot_general.48), kind=kOutput, calls=%fused_computation.6 | convolution fusion | flops 134283264 | bytes 4390912 | tf_op jit(solution)/shard_map/dot_general | solution.py:158
  88.1 0.0 reduce-scatter.2.cloned.1.call-update
  88.1 0.1 copy.82
  88.2 0.1 mul.251
  88.3 22.2 %reduce-scatter.2.cloned.1.call-done = bf16[8,4,512]{2,0,1:T(8,128)(2,1)} async-done(((bf16[8,4,2048]{2,0,1:T(8,128)(2,1)}), bf16[8,4,512]{2,0,1:T(8,128)(2,1)}) %reduce-scatter.2.cloned.1.call-update) | async-done | bytes 32784 | tf_op jit(solution)/shard_map/reduce_scatter | solution.py:161
  110.5 1.4 %copy.70 = bf16[8,4,512]{2,1,0:T(4,128)(2,1)} copy(bf16[8,4,512]{2,0,1:T(8,128)(2,1)} %reduce-scatter.2.cloned.1.call-done) | data formatting | bytes 65536 | tf_op jit(solution)/shard_map/reduce_scatter | solution.py:161
  111.9 4.6 %all-to-all-start.4 = ((bf16[8,4,512]{2,1,0:T(4,128)(2,1)}), bf16[8,4,512]{2,1,0:T(4,128)(2,1)S(1)}, u32[]{:S(2)}, u32[]{:S(2)}) async-start(bf16[8,4,512]{2,1,0:T(4,128)(2,1)} %copy.70), calls=%async_computation.5 | async-start | bytes 65536 | tf_op jit(solution)/shard_map/all_to_all | solution.py:164
  116.5 0.6 multiply_convert_fusion.1
  117.1 0.6 reshape.364
  117.7 4.5 %all-to-all-done.4 = bf16[8,4,512]{2,1,0:T(4,128)(2,1)S(1)} async-done(((bf16[8,4,512]{2,1,0:T(4,128)(2,1)}), bf16[8,4,512]{2,1,0:T(4,128)(2,1)S(1)}, u32[]{:S(2)}, u32[]{:S(2)}) %all-to-all-start.4) | async-done | bytes 32800 | tf_op jit(solution)/shard_map/all_to_all | solution.py:164
  122.2 0.8 fusion.17
  (46 shorter events, 0.4 us)
Async XLA Ops:
  7.2 10.9 %copy-start = (bf16[2048,512]{1,0:T(8,128)(2,1)S(1)}, bf16[2048,512]{1,0:T(8,128)(2,1)}, u32[]{:S(2)}) copy-start(bf16[2048,512]{1,0:T(8,128)(2,1)} %param.30) | copy-start | bytes 6291460
  7.2 16.3 %copy-start.6 = (s32[4,2]{0,1:T(2,128)S(1)}, s32[4,2]{0,1:T(2,128)}, u32[]{:S(2)}) copy-start(s32[4,2]{0,1:T(2,128)} %param.33) | copy-start | bytes 100
  20.2 12.1 %all-to-all-start.1 = ((bf16[4,2,256]{2,1,0:T(2,128)(2,1)}), bf16[4,2,256]{2,1,0:T(2,128)(2,1)S(1)}, u32[]{:S(2)}, u32[]{:S(2)}) async-start(bf16[4,2,256]{2,1,0:T(2,128)(2,1)} %reshape.396), calls=%async_computation.1 | async-start | bytes 8192 | tf_op jit(solution)/shard_map/all_to_all | solution.py:127
  23.7 2.8 %copy-start.2 = (bf16[2048,512]{1,0:T(8,128)(2,1)S(1)}, bf16[2048,512]{1,0:T(8,128)(2,1)}, u32[]{:S(2)}) copy-start(bf16[2048,512]{1,0:T(8,128)(2,1)} %param.31) | copy-start | bytes 6291460
  23.7 3.6 %copy-start.7 = (f32[4,2]{0,1:T(2,128)S(1)}, f32[4,2]{0,1:T(2,128)}, u32[]{:S(2)}) copy-start(f32[4,2]{0,1:T(2,128)} %param.34) | copy-start | bytes 100
  26.5 18.2 %copy-start.9 = (f32[128]{0:T(128)S(1)}, f32[128]{0:T(128)}, u32[]{:S(2)}) copy-start(f32[128]{0:T(128)} %param.25) | copy-start | bytes 1540
  26.5 18.2 %copy-start.10 = (f32[128]{0:T(128)S(1)}, f32[128]{0:T(128)}, u32[]{:S(2)}) copy-start(f32[128]{0:T(128)} %param.26) | copy-start | bytes 1540
  26.9 19.0 %copy-start.5 = (f32[8]{0:T(128)S(1)}, f32[8]{0:T(128)}, u32[]{:S(2)}) copy-start(f32[8]{0:T(128)} %param.23) | copy-start | bytes 100
  26.9 23.8 %copy-start.8 = (f32[256]{0:T(256)S(1)}, f32[256]{0:T(256)}, u32[]{:S(2)}) copy-start(f32[256]{0:T(256)} %param.27) | copy-start | bytes 3076
  28.9 29.2 %copy-start.3 = (bf16[4,512]{1,0:T(4,128)(2,1)S(1)}, bf16[4,512]{1,0:T(4,128)(2,1)}, u32[]{:S(2)}) copy-start(bf16[4,512]{1,0:T(4,128)(2,1)} %param.19) | copy-start | bytes 12292
  32.3 8.8 %all-to-all-start = ((bf16[4,2,256]{2,1,0:T(2,128)(2,1)}), bf16[4,2,256]{2,1,0:T(2,128)(2,1)S(1)}, u32[]{:S(2)}, u32[]{:S(2)}) async-start(bf16[4,2,256]{2,1,0:T(2,128)(2,1)} %reshape.394), calls=%async_computation | async-start | bytes 8192 | tf_op jit(solution)/shard_map/all_to_all | solution.py:126
  41.1 7.9 %all-to-all-start.2 = ((bf16[4,2,256]{2,1,0:T(2,128)(2,1)}), bf16[4,2,256]{2,1,0:T(2,128)(2,1)S(1)}, u32[]{:S(2)}, u32[]{:S(2)}) async-start(bf16[4,2,256]{2,1,0:T(2,128)(2,1)} %reshape.392), calls=%async_computation.2 | async-start | bytes 8192 | tf_op jit(solution)/shard_map/all_to_all | solution.py:128
  44.4 66.1 %reduce-scatter.2.cloned.1.call-start = ((), (), s32[]{:S(2)}) async-start(), calls=%async_computation.6 | async-start | bytes 163840 | tf_op jit(solution)/shard_map/reduce_scatter | solution.py:161
  45.0 23.3 %copy-start.4 = (f32[2048]{0:T(1024)S(1)}, f32[2048]{0:T(1024)}, u32[]{:S(2)}) copy-start(f32[2048]{0:T(1024)} %param.28) | copy-start | bytes 24580
  80.1 3.5 %copy-start.1 = (bf16[1,2048,1024]{2,1,0:T(8,128)(2,1)S(1)}, bf16[1,2048,1024]{2,1,0:T(8,128)(2,1)}, u32[]{:S(2)}) copy-start(bf16[1,2048,1024]{2,1,0:T(8,128)(2,1)} %param.36) | copy-start | bytes 12582916
  111.9 10.3 %all-to-all-start.4 = ((bf16[8,4,512]{2,1,0:T(4,128)(2,1)}), bf16[8,4,512]{2,1,0:T(4,128)(2,1)S(1)}, u32[]{:S(2)}, u32[]{:S(2)}) async-start(bf16[8,4,512]{2,1,0:T(4,128)(2,1)} %copy.70), calls=%async_computation.5 | async-start | bytes 65536 | tf_op jit(solution)/shard_map/all_to_all | solution.py:164
Sparse Core Ops, SparseCore 0:
  88.2 22.2 reduce-scatter.1
